TPU v7x, 32 devices: a whole 2x2x4 slice. The times are simulated.
32 devices in a mesh: sp: 8 (over z, y), tp: 4 (over x, core).
Axes of the slice: x: 2, y: 2, z: 4, core: 2. Of those that a mesh axis runs over, the one named last changes fastest.
Arguments:
- tokens: bfloat16 [2048, 2048], P('sp', 'tp'), may hold values from -19 to 250
- in_gain: bfloat16 [2048], replicated, may hold values from 0.099609375 to 1.8984375
- w_glu_value: bfloat16 [2048, 512], P(None, 'tp'), may hold values from -0.125 to 0.125
- w_glu_gate: bfloat16 [2048, 512], P(None, 'tp'), may hold values from -0.125 to 0.125
- w_query: bfloat16 [2048, 1024], P(None, 'tp'), may hold values from -1 to 1
- w_key: bfloat16 [2048, 512], P(None, 'tp'), may hold values from -1 to 1
- w_value: bfloat16 [2048, 512], P(None, 'tp'), may hold values from -0.125 to 0.125
- w_gate_conv: bfloat16 [2048, 512], P(None, 'tp'), may hold values from -0.125 to 0.125
- w_gate_attn: bfloat16 [2048, 1024], P(None, 'tp'), may hold values from -0.125 to 0.125
- conv_weight: bfloat16 [31, 512], P(None, 'tp'), may hold values from -4.6 to 4.6
- conv_gain: float32 [512], P('tp'), may hold values from 0.1 to 1.9
- lam: float32 [8], P('tp'), may hold values from 0.3 to 0.8
- head_gain: float32 [128], replicated, may hold values from 0.1 to 1.9
- out_conv: bfloat16 [512, 2048], P('tp'), may hold values from -0.15625 to 0.15625
- out_attn: bfloat16 [1024, 2048], P('tp'), may hold values from -0.15625 to 0.15625
Outputs:
- mixed: bfloat16 [2048, 2048], P(('sp', 'tp'))
All inputs are finite; a program needn't handle non-finite values.
Results may differ from a plain program's by a relative error of at most 0.017.
The roundings to bfloat16 on the way count: a program that leaves them out, or rounds other values in their place, can miss the bound.
Values may be sent and summed in bfloat16 or wider, within the bound.
A program may use at most 128 MiB of HBM per device.

v0:
```python
import math

import jax
import jax.numpy as jnp
from jax import lax
from jax.sharding import PartitionSpec as P

D = 2048
CONV = 512
QK = 64
VDIM = 128
WIDTH = 31


EPSILON = 1e-06
NEG_BIG = -1e30
HEAD_SCALE = 0.8


def shifted(x, axis, by):
    count = lax.axis_size(axis)
    pairs = [(i, i + by) for i in range(count) if 0 <= i + by < count]
    return lax.ppermute(x, axis, pairs)


def local(
    tokens,
    in_gain,
    w_glu_value,
    w_glu_gate,
    w_query,
    w_key,
    w_value,
    w_gate_conv,
    w_gate_attn,
    conv_weight,
    conv_gain,
    lam,
    head_gain,
    out_conv,
    out_attn,
):
    tok_rows = tokens.shape[0]
    weights = (w_glu_value, w_glu_gate, w_query, w_key, w_value, w_gate_conv, w_gate_attn)
    widened = lax.all_gather(tokens, "tp", axis=1, tiled=True).astype(jnp.float32)
    gain_part = in_gain.astype(jnp.float32)
    scaled = (widened * gain_part[None, :]).astype(jnp.bfloat16)
    updated = tuple(
        (jnp.dot(scaled, weight, preferred_element_type=jnp.float32) for weight in weights)
    )
    squares = jnp.sum(widened * widened, axis=1)
    inv_rms = lax.rsqrt(squares / D + EPSILON)[:, None]
    glu_value, glu_gate, query, key, value, gate_conv, gate_attn = [
        (total * inv_rms).astype(jnp.bfloat16) for total in updated
    ]
    glued = (glu_value.astype(jnp.float32) * jax.nn.sigmoid(glu_gate.astype(jnp.float32))).astype(
        jnp.bfloat16
    )
    tail_rows = WIDTH - 1
    last_rows = glued[tok_rows - tail_rows :]
    conv_local = glued.shape[1]
    kv_local = key.shape[1] // (2 * QK)
    heads_local = lam.shape[0]
    group = heads_local // kv_local
    my_index = lax.axis_index("sp")
    my_start = my_index * tok_rows
    scale_factor = 1.0 / math.sqrt(QK)
    query_groups = [
        (
            query.reshape(tok_rows, kv_local, group, 2, QK),
            my_start + jnp.arange(tok_rows, dtype=jnp.int32),
        )
    ]
    start_attn = tuple(
        (
            (
                jnp.full((kv_local, group, 2, rows_of.shape[0]), NEG_BIG, jnp.float32),
                jnp.zeros((kv_local, group, 2, rows_of.shape[0]), jnp.float32),
                jnp.zeros((kv_local, group, 2, rows_of.shape[0], VDIM), jnp.float32),
            )
            for rows_of, unused_pos in query_groups
        )
    )
    key_piece = lax.all_gather(key, "sp", axis=0, tiled=True)
    value_piece = lax.all_gather(value, "sp", axis=0, tiled=True)
    shards = key_piece.shape[0] // tok_rows
    stacked_keys = key_piece.reshape(shards, tok_rows, kv_local, 2, QK)
    stacked_values = value_piece.reshape(shards, tok_rows, kv_local, VDIM)
    firsts = tok_rows * jnp.arange(shards, dtype=jnp.int32)

    def visit(states, inputs):
        key_shard, value_shard, first = inputs
        key_pos = first + jnp.arange(tok_rows, dtype=jnp.int32)
        updated_states = []
        for (query_rows, query_pos), current_state in zip(query_groups, states):

            def update(current, query_rows=query_rows, query_pos=query_pos):
                maxima, totals, summed = current
                scores = (
                    jnp.einsum(
                        "qagcd,kacd->agcqk",
                        query_rows,
                        key_shard,
                        preferred_element_type=jnp.float32,
                    )
                    * scale_factor
                )
                allowed = key_pos[None, :] <= query_pos[:, None]
                scores = jnp.where(allowed, scores, NEG_BIG)
                new_max = jnp.maximum(maxima, jnp.max(scores, axis=4))
                factor = jnp.exp(maxima - new_max)
                expd = jnp.exp(scores - new_max[..., None])
                totals = totals * factor + jnp.sum(expd, axis=4)
                summed = summed * factor[..., None] + jnp.einsum(
                    "agcqk,kav->agcqv",
                    expd.astype(jnp.bfloat16),
                    value_shard,
                    preferred_element_type=jnp.float32,
                )
                return (new_max, totals, summed)

            def keep(current):
                return current

            query_last = query_pos[0] + query_pos.shape[0] - 1
            updated_states.append(lax.cond(first <= query_last, update, keep, current_state))
        return (tuple(updated_states), None)

    result, unused = lax.scan(visit, start_attn, (stacked_keys, stacked_values, firsts))
    states = result
    maxima, totals, summed = states[0]
    output = (
        summed[:, :, 0] / totals[:, :, 0][..., None]
        - lam.reshape(kv_local, group)[:, :, None, None]
        * summed[:, :, 1]
        / totals[:, :, 1][..., None]
    )
    normed = output * lax.rsqrt(jnp.mean(output * output, axis=3, keepdims=True) + EPSILON)
    normed = normed * head_gain[None, None, None, :] * HEAD_SCALE
    laid = jnp.transpose(normed, (2, 0, 1, 3)).reshape(normed.shape[2], heads_local * VDIM)
    y_attn = (laid * jax.nn.silu(gate_attn.astype(jnp.float32))).astype(jnp.bfloat16)
    previous = shifted(last_rows, "sp", 1)
    padded = jnp.concatenate([previous, glued], axis=0).astype(jnp.float32)
    taps = conv_weight.astype(jnp.float32)
    conv = jnp.zeros((tok_rows, conv_local), jnp.float32)
    for offset in range(WIDTH):
        conv = conv + padded[offset : offset + tok_rows] * taps[offset][None, :]
    total_sq = lax.psum(jnp.sum(conv * conv, axis=1), "tp")
    normed = conv * lax.rsqrt(total_sq / CONV + EPSILON)[:, None] * conv_gain[None, :]
    y_conv = (jax.nn.silu(normed) * jax.nn.silu(gate_conv.astype(jnp.float32))).astype(jnp.bfloat16)
    return lax.psum_scatter(
        (
            jnp.dot(y_conv, out_conv, preferred_element_type=jnp.float32)
            + jnp.dot(y_attn, out_attn, preferred_element_type=jnp.float32)
        ).astype(jnp.bfloat16),
        "tp",
        scatter_dimension=0,
        tiled=True,
    )


def solution(mesh):
    in_specs = (
        P("sp", "tp"),
        P(),
        P(None, "tp"),
        P(None, "tp"),
        P(None, "tp"),
        P(None, "tp"),
        P(None, "tp"),
        P(None, "tp"),
        P(None, "tp"),
        P(None, "tp"),
        P("tp"),
        P("tp"),
        P(),
        P("tp", None),
        P("tp", None),
    )
    out_specs = P(("sp", "tp"), None)
    return jax.shard_map(local, mesh=mesh, in_specs=in_specs, out_specs=out_specs, check_vma=False)
```

profile of v0, /device:TPU:25, one launch (start us, length us, event | category | flops | bytes accessed | tf_op | source)
XLA Modules:
  0.0 184.7 jit_solution(6918326451705439415)
XLA Ops:
  9.8 17.2 %all-gather.2.cloned.1.call-done = bf16[256,2048]{1,0:T(8,128)(2,1)} async-done(((bf16[256,512]{1,0:T(8,128)(2,1)}), bf16[256,2048]{1,0:T(8,128)(2,1)}) %all-gather.2.cloned.1.call-update) | async-done | bytes 1048592 | tf_op jit(solution)/shard_map/all_gather | solution.py:45
  27.0 1.5 fusion.19
  28.5 1.8 fusion.35
  30.3 24.9 %all_gather.10 = bf16[2048,128]{1,0:T(8,128)(2,1)} all-gather(bf16[256,128]{1,0:T(8,128)(2,1)S(1)} %fusion.35), channel_id=1, replica_groups=mesh['sp'=8,'tp'=4] {'sp'}, dimensions={0}, use_global_device_ids=true | all-gather | bytes 589824 | tf_op jit(solution)/shard_map/all_gather | solution.py:84
  55.2 2.4 %reshape.159 = bf16[8,256,1,2,64]{4,3,1,0,2:T(2,128)(2,1)S(1)} reshape(bf16[2048,128]{1,0:T(8,128)(2,1)} %all_gather.10) | data formatting | bytes 1048576 | tf_op jit(solution)/shard_map/reshape | solution.py:87
  57.6 1.8 copy.27
  59.4 1.6 fusion.36
  61.0 25.8 %all_gather.11 = bf16[2048,128]{1,0:T(8,128)(2,1)S(1)} all-gather(bf16[256,128]{1,0:T(8,128)(2,1)S(1)} %fusion.36), channel_id=1, replica_groups=mesh['sp'=8,'tp'=4] {'sp'}, dimensions={0}, use_global_device_ids=true | all-gather | bytes 589824 | tf_op jit(solution)/shard_map/all_gather | solution.py:85
  87.4 30.4 %while.17 = (s32[]{:T(128)}, f32[1,2,2,256]{3,1,2,0:T(2,128)S(1)}, f32[1,2,2,256]{3,1,2,0:T(2,128)S(1)}, f32[1,2,2,256,128]{4,3,2,1,0:T(8,128)S(1)}, s32[8]{0:T(...) while((s32[]{:T(128)}, f32[1,2,2,256]{3,1,2,0:T(2,128)S(1)}, ...), condition=%wide.region_8.9_spmd.clone, body=%wide.region_3.8_spmd.clone.sunk | while | flops 102567424 | bytes 4665123 | solution.py:129
  88.8 2.8 %conditional.3 = ((f32[1,2,2,256]{3,1,2,0:T(2,128)S(1)}, f32[1,2,2,256]{3,1,2,0:T(2,128)S(1)}, f32[1,2,2,256,128]{4,3,2,1,0:T(8,128)S(1)})) conditional(s32[]{:T(128)} %convert_element_type.190, (f32[1,2,2,256]{3,1,2,0:T(2,128)S(1)}, f32[1,2,2,256]{3,1,2,0:T(2,128)S(1)}, f32[1,2,2,256,128]{4,3,2,1,0:T(8,128)S(1)}) %tuple.82, (s32[]{:T(128)}, ...), branch_computations={%region_4.4_spmd, %region_5.7_spmd} | conditional | flops 102567424 | bytes 4663852 | solution.py:126
  89.6 1.2 fusion.99
  92.9 2.8 %conditional.3 = ((f32[1,2,2,256]{3,1,2,0:T(2,128)S(1)}, f32[1,2,2,256]{3,1,2,0:T(2,128)S(1)}, f32[1,2,2,256,128]{4,3,2,1,0:T(8,128)S(1)})) conditional(s32[]{:T(128)} %convert_element_type.190, (f32[1,2,2,256]{3,1,2,0:T(2,128)S(1)}, f32[1,2,2,256]{3,1,2,0:T(2,128)S(1)}, f32[1,2,2,256,128]{4,3,2,1,0:T(8,128)S(1)}) %tuple.82, (s32[]{:T(128)}, ...), branch_computations={%region_4.4_spmd, %region_5.7_spmd} | conditional | flops 102567424 | bytes 4663852 | solution.py:126
  97.1 2.8 %conditional.3 = ((f32[1,2,2,256]{3,1,2,0:T(2,128)S(1)}, f32[1,2,2,256]{3,1,2,0:T(2,128)S(1)}, f32[1,2,2,256,128]{4,3,2,1,0:T(8,128)S(1)})) conditional(s32[]{:T(128)} %convert_element_type.190, (f32[1,2,2,256]{3,1,2,0:T(2,128)S(1)}, f32[1,2,2,256]{3,1,2,0:T(2,128)S(1)}, f32[1,2,2,256,128]{4,3,2,1,0:T(8,128)S(1)}) %tuple.82, (s32[]{:T(128)}, ...), branch_computations={%region_4.4_spmd, %region_5.7_spmd} | conditional | flops 102567424 | bytes 4663852 | solution.py:126
  97.9 1.2 fusion.99
  101.2 2.8 %conditional.3 = ((f32[1,2,2,256]{3,1,2,0:T(2,128)S(1)}, f32[1,2,2,256]{3,1,2,0:T(2,128)S(1)}, f32[1,2,2,256,128]{4,3,2,1,0:T(8,128)S(1)})) conditional(s32[]{:T(128)} %convert_element_type.190, (f32[1,2,2,256]{3,1,2,0:T(2,128)S(1)}, f32[1,2,2,256]{3,1,2,0:T(2,128)S(1)}, f32[1,2,2,256,128]{4,3,2,1,0:T(8,128)S(1)}) %tuple.82, (s32[]{:T(128)}, ...), branch_computations={%region_4.4_spmd, %region_5.7_spmd} | conditional | flops 102567424 | bytes 4663852 | solution.py:126
  105.4 2.8 %conditional.3 = ((f32[1,2,2,256]{3,1,2,0:T(2,128)S(1)}, f32[1,2,2,256]{3,1,2,0:T(2,128)S(1)}, f32[1,2,2,256,128]{4,3,2,1,0:T(8,128)S(1)})) conditional(s32[]{:T(128)} %convert_element_type.190, (f32[1,2,2,256]{3,1,2,0:T(2,128)S(1)}, f32[1,2,2,256]{3,1,2,0:T(2,128)S(1)}, f32[1,2,2,256,128]{4,3,2,1,0:T(8,128)S(1)}) %tuple.82, (s32[]{:T(128)}, ...), branch_computations={%region_4.4_spmd, %region_5.7_spmd} | conditional | flops 102567424 | bytes 4663852 | solution.py:126
  109.5 2.8 %conditional.3 = ((f32[1,2,2,256]{3,1,2,0:T(2,128)S(1)}, f32[1,2,2,256]{3,1,2,0:T(2,128)S(1)}, f32[1,2,2,256,128]{4,3,2,1,0:T(8,128)S(1)})) conditional(s32[]{:T(128)} %convert_element_type.190, (f32[1,2,2,256]{3,1,2,0:T(2,128)S(1)}, f32[1,2,2,256]{3,1,2,0:T(2,128)S(1)}, f32[1,2,2,256,128]{4,3,2,1,0:T(8,128)S(1)}) %tuple.82, (s32[]{:T(128)}, ...), branch_computations={%region_4.4_spmd, %region_5.7_spmd} | conditional | flops 102567424 | bytes 4663852 | solution.py:126
  113.7 2.8 %conditional.3 = ((f32[1,2,2,256]{3,1,2,0:T(2,128)S(1)}, f32[1,2,2,256]{3,1,2,0:T(2,128)S(1)}, f32[1,2,2,256,128]{4,3,2,1,0:T(8,128)S(1)})) conditional(s32[]{:T(128)} %convert_element_type.190, (f32[1,2,2,256]{3,1,2,0:T(2,128)S(1)}, f32[1,2,2,256]{3,1,2,0:T(2,128)S(1)}, f32[1,2,2,256,128]{4,3,2,1,0:T(8,128)S(1)}) %tuple.82, (s32[]{:T(128)}, ...), branch_computations={%region_4.4_spmd, %region_5.7_spmd} | conditional | flops 102567424 | bytes 4663852 | solution.py:126
  118.5 1.6 fusion.32
  120.6 7.3 %collective-permute-start = (bf16[30,128]{1,0:T(8,128)(2,1)S(1)}, bf16[30,128]{1,0:T(8,128)(2,1)S(1)}, u32[]{:S(2)}, u32[]{:S(2)}) collective-permute-start(bf16[30,128]{1,0:T(8,128)(2,1)S(1)} %slice.274), channel_id=1, source_target_pairs={{0,4},{4,8},{8,12},{12,16},{16,20},{20,24},{24,28},{1,5},{5,9},{9,... | collective-permute-start | bytes 23048 | tf_op jit(solution)/shard_map/ppermute | solution.py:23
  129.2 19.1 %psum.7 = f32[256]{0:T(256)S(1)} all-reduce(f32[256]{0:T(256)S(1)} %get-tuple-element.287), channel_id=1, replica_groups=mesh['sp'=8,'tp'=4] {'tp'}, use_global_device_ids=true, to_apply=%region_2.3 | all-reduce | flops 256 | bytes 2048 | tf_op jit(solution)/shard_map/psum | solution.py:148
  148.4 2.3 %fusion.83 = f32[256,2048]{1,0:T(8,128)S(1)} fusion(bf16[128,2048]{1,0:T(8,128)(2,1)} %param.32, bf16[2048,128]{1,0:T(8,128)(2,1)} %param.26, bf16[256,2048]{1,0:T(8,128)(2,1)} %all-gather.2.cloned.1.call-done, f32[2048]{0:T(1024)S(1)} %convert_element_type.71, f32[256,128]{1,0:T(8,128)S(1)} %get-tuple-element.288, f32[128]{0:T(128)S(1)} %copy-done.3, ...), kind=kOutput, calls=%fused_computation.126 | convolution fusion | flops 270499840 | bytes 4336128 | tf_op jit(solution)/shard_map/dot_general | solution.py:153
  150.7 1.4 fusion.17
  152.2 25.7 %reduce-scatter.2.cloned.1.call-done = bf16[64,2048]{1,0:T(8,128)(2,1)} async-done(((bf16[256,2048]{1,0:T(8,128)(2,1)}), bf16[64,2048]{1,0:T(8,128)(2,1)}) %reduce-scatter.2.cloned.1.call-update) | async-done | bytes 262160 | tf_op jit(solution)/shard_map/reduce_scatter | solution.py:151
  (123 shorter events, 27.6 us)
Async XLA Ops:
  6.5 144.2 %copy-start = (bf16[256,2048]{1,0:T(8,128)(2,1)S(1)}, bf16[256,2048]{1,0:T(8,128)(2,1)}, u32[]{:S(2)}) copy-start(bf16[256,2048]{1,0:T(8,128)(2,1)} %param.33) | copy-start | bytes 3145732
  6.5 20.5 %all-gather.2.cloned.1.call-start = ((), (), s32[]{:S(2)}) async-start(), calls=%async_computation.1 | async-start | bytes 1310720 | tf_op jit(solution)/shard_map/all_gather | solution.py:45
  7.3 170.6 %reduce-scatter.2.cloned.1.call-start = ((), (), s32[]{:S(2)}) async-start(), calls=%async_computation.2 | async-start | bytes 1310720 | tf_op jit(solution)/shard_map/reduce_scatter | solution.py:151
  30.3 29.1 %copy-start.1 = (bf16[256,2048]{1,0:T(8,128)(2,1)S(1)}, bf16[256,2048]{1,0:T(8,128)(2,1)}, u32[]{:S(2)}) copy-start(bf16[256,2048]{1,0:T(8,128)(2,1)} %all-gather.2.cloned.1.call-done) | copy-start | bytes 3145732
  59.4 27.3 %copy-start.5 = (bf16[2048,256]{1,0:T(8,128)(2,1)S(1)}, bf16[2048,256]{1,0:T(8,128)(2,1)}, u32[]{:S(2)}) copy-start(bf16[2048,256]{1,0:T(8,128)(2,1)} %param.23) | copy-start | bytes 3145732
  87.4 30.5 %copy-start.4 = (f32[2]{0:T(128)S(1)}, f32[2]{0:T(128)}, u32[]{:S(2)}) copy-start(f32[2]{0:T(128)} %param.30) | copy-start | bytes 28
  87.4 30.8 %copy-start.2 = (f32[128]{0:T(128)S(1)}, f32[128]{0:T(128)}, u32[]{:S(2)}) copy-start(f32[128]{0:T(128)} %param.31) | copy-start | bytes 1540
  117.9 2.2 %copy-start.7 = (bf16[2048,128]{1,0:T(8,128)(2,1)S(1)}, bf16[2048,128]{1,0:T(8,128)(2,1)}, u32[]{:S(2)}) copy-start(bf16[2048,128]{1,0:T(8,128)(2,1)} %param.21) | copy-start | bytes 1572868
  118.5 9.3 %copy-start.6 = (bf16[2048,256]{1,0:T(8,128)(2,1)S(1)}, bf16[2048,256]{1,0:T(8,128)(2,1)}, u32[]{:S(2)}) copy-start(bf16[2048,256]{1,0:T(8,128)(2,1)} %param.27) | copy-start | bytes 3145732
  120.6 8.1 %collective-permute-start = (bf16[30,128]{1,0:T(8,128)(2,1)S(1)}, bf16[30,128]{1,0:T(8,128)(2,1)S(1)}, u32[]{:S(2)}, u32[]{:S(2)}) collective-permute-start(bf16[30,128]{1,0:T(8,128)(2,1)S(1)} %slice.274), channel_id=1, source_target_pairs={{0,4},{4,8},{8,12},{12,16},{16,20},{20,24},{24,28},{1,5},{5,9},{9,... | collective-permute-start | bytes 23048 | tf_op jit(solution)/shard_map/ppermute | solution.py:23
  128.7 19.7 %copy-start.3 = (f32[128]{0:T(128)S(1)}, f32[128]{0:T(128)}, u32[]{:S(2)}) copy-start(f32[128]{0:T(128)} %param.29) | copy-start | bytes 1540
Sparse Core Ops, SparseCore 0:
  8.9 18.0 all-gather.1
  152.3 25.5 reduce-scatter.1
where the time goes:
time: 187 us; the launch traced here: 185 us
  blocking collectives  69.8 us (37%)
  waiting for transfers between devices  43.8 us (23%)
  matrix products  22.3 us (12%)
  between operations  14.2 us (8%)
  other arithmetic  10.9 us (6%)
  local copies, waits for them, and re-layouts  10.2 us (5%)
  starting transfers between devices  7.33 us (4%)
  loops' own time  6.15 us (3%)
    all_gather x1, blocking collectives, local(): value_piece = lax.all_gather(value, 'sp', axis=0, tiled=True)  25.8 us
    reduce_scatter x1, waiting for transfers between devices, local(): lax.psum_scatter((jnp.dot(y_conv, out_conv, preferred_element_type=jnp.fl...  25.7 us
    all_gather x1, blocking collectives, local(): key_piece = lax.all_gather(key, 'sp', axis=0, tiled=True)  24.9 us
    psum x1, blocking collectives, local(): total_sq = lax.psum(jnp.sum(conv * conv, axis=1), 'tp')  19.1 us
    all_gather x1, waiting for transfers between devices, local(): lax.all_gather(tokens, 'tp', axis=1, tiled=True).astype(jnp.float32)  17.2 us
    dot_general x7, matrix products, update(): jnp.einsum('qagcd,kacd->agcqk', query_rows, key_shard, preferred_element_...  8.44 us
    ppermute x1, starting transfers between devices, shifted(): return lax.ppermute(x, axis, pairs)  7.29 us
    dot_general x6, matrix products, local(): jnp.dot(scaled, weight, preferred_element_type=jnp.float32)  6.52 us
  transfers between devices with their start and end apart: 3, of which 3 were waited for; matrix products, arithmetic and copies ran while one was open for 1% of the time, Pallas kernels for 0%

commit v1 on v0

v1 whole, which is shorter than its diff:
```python
import functools
import math

import jax
import jax.numpy as jnp
from jax import lax
from jax.experimental import pallas as pl
from jax.experimental.pallas import tpu as pltpu
from jax.sharding import PartitionSpec as P

EPSILON = 1e-06
NEG_BIG = -1e30
HEAD_SCALE = 0.8
QK = 64
VDIM = 128
MESH = pl.DeviceIdType.MESH
F32 = jnp.float32
BF16 = jnp.bfloat16
PIECES = 4
PAD = 32


def dot(a, b, ca=1, cb=0, precision=None):
    return lax.dot_general(
        a, b, (((ca,), (cb,)), ((), ())), preferred_element_type=F32, precision=precision
    )


def kernel(
    n_sp,
    n_tp,
    tok,
    gain,
    w_glu_value,
    w_glu_gate,
    w_query,
    w_key,
    w_value,
    w_gate_conv,
    w_gate_attn,
    taps_ref,
    conv_gain,
    lam,
    head_gain,
    out_conv,
    out_attn,
    out,
    w_all,
    w_out,
    tokbuf,
    acc,
    kbuf,
    vbuf,
    q4,
    m_ref,
    l_ref,
    o_ref,
    gl,
    tail_out,
    tail_in,
    sq_out,
    sq_in,
    ybuf,
    a_out,
    a_own,
    a_in,
    x_out,
    x_in,
    b_out,
    b_own,
    b_in,
    w_sem,
    tok_send,
    tok_recv,
    kv_recv,
    up_send,
    side_send,
    tail_sem,
    sq_send,
    sq_recv,
    a_sem,
    x_sem,
    b_sem,
):
    rows, depth = tok.shape
    width = depth * n_tp
    s = lax.axis_index("sp")
    t = lax.axis_index("tp")
    core = t % 2
    p1 = t + 1 - 2 * core
    p2 = (t + 2) % n_tp
    p3 = (p1 + 2) % n_tp
    y = s % 2
    z = s // 2
    mate = s + 1 - 2 * y
    has_up = s + 2 < n_sp

    weights = (w_key, w_value, w_glu_value, w_glu_gate, w_query, w_gate_conv, w_gate_attn)
    spans = []
    at = 0
    loads = []
    for i, w in enumerate(weights):
        cols = w.shape[1]
        spans.append((at, at + cols))
        loads.append(pltpu.make_async_copy(w, w_all.at[:, at : at + cols], w_sem.at[i]))
        at += cols
    total_cols = at
    at = 0
    out_loads = []
    for i, w in enumerate((out_conv, out_attn)):
        r = w.shape[0]
        out_loads.append(
            pltpu.make_async_copy(w, w_out.at[at : at + r, :], w_sem.at[len(weights) + i])
        )
        at += r
    for copy in loads + out_loads:
        copy.start()

    def tp_copy(src, dst, send, recv, to):
        return pltpu.make_async_remote_copy(
            src_ref=src, dst_ref=dst, send_sem=send, recv_sem=recv,
            device_id={"tp": to}, device_id_type=MESH,
        )

    def sp_copy(src, dst, send, recv, to):
        return pltpu.make_async_remote_copy(
            src_ref=src, dst_ref=dst, send_sem=send, recv_sem=recv,
            device_id={"sp": to}, device_id_type=MESH,
        )

    barrier = pltpu.get_barrier_semaphore()
    for peer in (p1, p2, p3):
        pl.semaphore_signal(barrier, inc=1, device_id={"tp": peer}, device_id_type=MESH)
    for by in (-2, -1, 1, 2):
        other = s + by

        @pl.when((other >= 0) & (other < n_sp))
        def _():
            pl.semaphore_signal(barrier, inc=1, device_id={"sp": other}, device_id_type=MESH)

    pl.semaphore_wait(barrier, 3 + jnp.minimum(s, 2) + jnp.minimum(n_sp - 1 - s, 2))

    half = rows // 2
    across = [
        tp_copy(
            tok.at[c * half : (c + 1) * half], tokbuf.at[1, c * half : (c + 1) * half],
            tok_send.at[c], tok_recv.at[c], p2,
        )
        for c in range(2)
    ]
    beside = tp_copy(tok, tokbuf.at[0], tok_send.at[2], tok_recv.at[2], p1)
    passed = [
        tp_copy(
            tokbuf.at[1, c * half : (c + 1) * half], tokbuf.at[2, c * half : (c + 1) * half],
            tok_send.at[3 + c], tok_recv.at[3 + c], p1,
        )
        for c in range(2)
    ]
    for copy in across:
        copy.start()
    beside.start()

    def prepare(x, owner):
        wide = x.astype(F32)
        first = pl.multiple_of(owner * depth, depth)
        g = gain[:, pl.ds(first, depth)].astype(F32)
        return (wide * g).astype(BF16), jnp.sum(wide * wide, axis=1, keepdims=True), first

    scaled, squares, first = prepare(tok[...], t)
    for copy in loads:
        copy.wait()
    acc[...] = dot(scaled, w_all[pl.ds(first, depth), :])
    beside.wait_recv()
    scaled, more, first = prepare(tokbuf[0], p1)
    squares = squares + more
    acc[...] += dot(scaled, w_all[pl.ds(first, depth), :])
    for c in range(2):
        across[c].wait_recv()
        passed[c].start()
    scaled, more, first = prepare(tokbuf[1], p2)
    squares = squares + more
    acc[...] += dot(scaled, w_all[pl.ds(first, depth), :])
    for c in range(2):
        passed[c].wait_recv()
    scaled, more, first = prepare(tokbuf[2], p3)
    squares = squares + more
    inv_rms = lax.rsqrt(squares / width + EPSILON)
    early = spans[3][1]
    acc[:, :early] += dot(scaled, w_all[pl.ds(first, depth), :early])

    def projected(i, lo=0, hi=None):
        hi = rows if hi is None else hi
        a, b = spans[i]
        return (acc[lo:hi, a:b] * inv_rms[lo:hi]).astype(BF16)

    def glue(lo, hi):
        value = projected(2, lo, hi).astype(F32)
        gate = projected(3, lo, hi).astype(F32)
        return (value * jax.nn.sigmoid(gate)).astype(BF16)

    tail_out[...] = glue(rows - PAD, rows)
    tail = sp_copy(tail_out, tail_in, tail_sem.at[0], tail_sem.at[1], s + 1)

    @pl.when(s + 1 < n_sp)
    def _():
        tail.start()

    def up(j, c):
        buf = (kbuf, vbuf)[c]
        return sp_copy(buf.at[j], buf.at[j], up_send.at[j, c], kv_recv.at[j, c], s + 2)

    def side(j, c):
        buf = (kbuf, vbuf)[c]
        return sp_copy(buf.at[j], buf.at[j], side_send.at[j, c], kv_recv.at[j, c], mate)

    kbuf[s] = projected(0)
    vbuf[s] = jnp.transpose(projected(1).astype(F32)).astype(BF16)
    for c in range(2):

        @pl.when(has_up)
        def _():
            up(s, c).start()

        @pl.when(y == 0)
        def _():
            side(s, c).start()

    acc[:, early:] += dot(scaled, w_all[pl.ds(first, depth), early:])
    query = projected(4).astype(F32) * (1.0 / math.sqrt(QK))
    heads = w_query.shape[1] // (2 * QK)
    lane = lax.broadcasted_iota(jnp.int32, (rows, 2 * QK), 1)
    for h in range(heads):
        qh = query[:, h * 2 * QK : (h + 1) * 2 * QK]
        for m in range(2):
            keep = (lane >= m * QK) & (lane < (m + 1) * QK)
            q4[2 * h + m] = jnp.where(keep, qh, 0.0).astype(BF16)
    gl[PAD:, :] = glue(0, rows).astype(F32)

    key_pos = lax.broadcasted_iota(jnp.int32, (rows, rows), 0)
    query_pos = lax.broadcasted_iota(jnp.int32, (rows, rows), 1)
    allowed = key_pos <= query_pos
    k = kbuf[s]
    v = vbuf[s]
    for i in range(2 * heads):
        scores = jnp.where(allowed, dot(k, q4[i], 1, 1), NEG_BIG)
        top = jnp.max(scores, axis=0, keepdims=True)
        e = jnp.exp(scores - top)
        m_ref[i] = top
        l_ref[i] = jnp.sum(e, axis=0, keepdims=True)
        o_ref[i] = dot(v, e.astype(BF16))

    @pl.when(s == 0)
    def _():
        gl[:PAD, :] = jnp.zeros((PAD, gl.shape[1]), F32)

    @pl.when(s > 0)
    def _():
        tail.wait_recv()
        gl[:PAD, :] = tail_in[...].astype(F32)

    n_taps = taps_ref.shape[0]
    taps = taps_ref[...].astype(F32)
    conv = jnp.zeros((rows, gl.shape[1]), F32)
    for j in range(n_taps):
        lo = PAD - (n_taps - 1) + j
        conv = conv + gl[lo : lo + rows, :] * taps[j : j + 1, :]
    ones = jnp.ones((8, conv.shape[1]), F32)
    high = lax.Precision.HIGHEST
    sq_out[...] = dot(ones, conv * conv, 1, 1, high)
    sq_copies = [
        tp_copy(sq_out, sq_in.at[i], sq_send.at[i], sq_recv.at[i], p)
        for i, p in enumerate((p1, p2, p3))
    ]
    for copy in sq_copies:
        copy.start()

    def visit(j):
        k = kbuf[j]
        v = vbuf[j]
        for i in range(2 * heads):
            scores = dot(k, q4[i], 1, 1)
            old = m_ref[i]
            top = jnp.maximum(old, jnp.max(scores, axis=0, keepdims=True))
            factor = jnp.exp(old - top)
            e = jnp.exp(scores - top)
            m_ref[i] = top
            l_ref[i] = l_ref[i] * factor + jnp.sum(e, axis=0, keepdims=True)
            o_ref[i] = o_ref[i] * factor + dot(v, e.astype(BF16))

    gate_conv = projected(5).astype(F32)
    for copy in sq_copies:
        copy.wait_recv()
    total_sq = sq_out[...] + sq_in[0] + sq_in[1] + sq_in[2]
    spread = jnp.full((8, conv.shape[1]), 0.125, F32)
    conv_all = conv.shape[1] * n_tp
    mean_sq = dot(total_sq, spread, 0, 0, high) / conv_all
    normed = conv * lax.rsqrt(mean_sq + EPSILON) * conv_gain[...]
    conv_local = conv.shape[1]
    ybuf[:, :conv_local] = (
        normed * jax.nn.sigmoid(normed) * (gate_conv * jax.nn.sigmoid(gate_conv))
    ).astype(BF16)

    @pl.when(y == 1)
    def _():
        for c in range(2):
            side(mate, c).wait_recv()
        visit(mate)

    def step(i, carry):
        k = i + 1
        j = s - 2 * k
        for c in range(2):
            up(j, c).wait_recv()

            @pl.when(has_up)
            def _():
                up(j, c).start()

            side(j, c).start()
        visit(j)
        other = mate - 2 * k
        for c in range(2):
            side(other, c).wait_recv()
        visit(other)
        return carry

    lax.fori_loop(0, z, step, 0)

    for h in range(heads):
        first_map = o_ref[2 * h] / l_ref[2 * h]
        second_map = o_ref[2 * h + 1] / l_ref[2 * h + 1]
        o = first_map - lam[h] * second_map
        n = o * lax.rsqrt(jnp.mean(o * o, axis=0, keepdims=True) + EPSILON)
        a, b = spans[6]
        lo = a + h * VDIM
        gate = (acc[:, lo : lo + VDIM] * inv_rms).astype(BF16).astype(F32)
        n = jnp.transpose(n) * head_gain[...] * HEAD_SCALE
        at = conv_local + h * VDIM
        ybuf[:, at : at + VDIM] = (n * (gate * jax.nn.sigmoid(gate))).astype(BF16)

    for copy in out_loads:
        copy.wait()
    part = rows // n_tp

    def block(p):
        return ybuf[pl.ds(pl.multiple_of(p * part, part), part), :]

    cols = w_out.shape[1] // PIECES
    far = jnp.concatenate([block(p3), block(p2)], axis=0)
    a_copies = []
    for c in range(PIECES):
        r = dot(far, w_out[:, c * cols : (c + 1) * cols]).astype(BF16)
        a_out[c] = r[:part]
        a_own[c] = r[part:]
        copy = tp_copy(a_out.at[c], a_in.at[c], a_sem.at[0, c], a_sem.at[1, c], p1)
        copy.start()
        a_copies.append(copy)
    x_copies = []
    for c in range(PIECES):
        a_copies[c].wait_recv()
        x_out[c] = (a_own[c].astype(F32) + a_in[c].astype(F32)).astype(BF16)
        copy = tp_copy(x_out.at[c], x_in.at[c], x_sem.at[0, c], x_sem.at[1, c], p2)
        copy.start()
        x_copies.append(copy)
    near = jnp.concatenate([block(p1), block(t)], axis=0)
    b_copies = []
    for c in range(PIECES):
        r = dot(near, w_out[:, c * cols : (c + 1) * cols]).astype(BF16)
        b_out[c] = r[:part]
        b_own[c] = r[part:]
        copy = tp_copy(b_out.at[c], b_in.at[c], b_sem.at[0, c], b_sem.at[1, c], p1)
        copy.start()
        b_copies.append(copy)
    for c in range(PIECES):
        b_copies[c].wait_recv()
        x_copies[c].wait_recv()
        out[:, c * cols : (c + 1) * cols] = (
            b_own[c].astype(F32) + b_in[c].astype(F32) + x_in[c].astype(F32)
        ).astype(BF16)

    for copy in across + [beside] + passed + sq_copies + a_copies + x_copies + b_copies:
        copy.wait_send()

    @pl.when(s + 1 < n_sp)
    def _():
        tail.wait_send()

    for c in range(2):

        @pl.when(has_up)
        def _():
            up(s, c).wait_send()

        @pl.when(y == 0)
        def _():
            side(s, c).wait_send()

    def drain(i, carry):
        j = s - 2 * (i + 1)
        for c in range(2):

            @pl.when(has_up)
            def _():
                up(j, c).wait_send()

            side(j, c).wait_send()
        return carry

    lax.fori_loop(0, z, drain, 0)


def local(n_sp, n_tp, *args):
    (tokens, in_gain, w_glu_value, w_glu_gate, w_query, w_key, w_value, w_gate_conv,
     w_gate_attn, conv_weight, conv_gain, lam, head_gain, out_conv, out_attn) = args
    rows, depth = tokens.shape
    width = depth * n_tp
    weights = (w_glu_value, w_glu_gate, w_query, w_key, w_value, w_gate_conv, w_gate_attn)
    total_cols = sum(w.shape[1] for w in weights)
    out_rows = out_conv.shape[0] + out_attn.shape[0]
    out_cols = out_conv.shape[1]
    conv_local = conv_weight.shape[1]
    heads = lam.shape[0]
    part = rows // n_tp
    cols = out_cols // PIECES
    vmem = pl.BlockSpec(memory_space=pltpu.VMEM)
    hbm = pl.BlockSpec(memory_space=pl.ANY)
    smem = pl.BlockSpec(memory_space=pltpu.SMEM)
    dma = pltpu.SemaphoreType.DMA
    piece = pltpu.VMEM((PIECES, part, cols), BF16)
    return pl.pallas_call(
        functools.partial(kernel, n_sp, n_tp),
        out_shape=jax.ShapeDtypeStruct((part, out_cols), BF16),
        in_specs=[vmem, vmem] + [hbm] * 7 + [vmem, vmem, smem, vmem, hbm, hbm],
        out_specs=vmem,
        scratch_shapes=[
            pltpu.VMEM((width, total_cols), BF16),
            pltpu.VMEM((out_rows, out_cols), BF16),
            pltpu.VMEM((3, rows, depth), BF16),
            pltpu.VMEM((rows, total_cols), F32),
            pltpu.VMEM((n_sp, rows, 2 * QK), BF16),
            pltpu.VMEM((n_sp, VDIM, rows), BF16),
            pltpu.VMEM((2 * heads, rows, 2 * QK), BF16),
            pltpu.VMEM((2 * heads, 1, rows), F32),
            pltpu.VMEM((2 * heads, 1, rows), F32),
            pltpu.VMEM((2 * heads, VDIM, rows), F32),
            pltpu.VMEM((PAD + rows, conv_local), F32),
            pltpu.VMEM((PAD, conv_local), BF16),
            pltpu.VMEM((PAD, conv_local), BF16),
            pltpu.VMEM((8, rows), F32),
            pltpu.VMEM((3, 8, rows), F32),
            pltpu.VMEM((rows, out_rows), BF16),
            piece, piece, piece, piece, piece, piece, piece, piece,
            dma((9,)),
            dma((5,)),
            dma((5,)),
            dma((n_sp, 2)),
            dma((n_sp, 2)),
            dma((n_sp, 2)),
            dma((2,)),
            dma((3,)),
            dma((3,)),
            dma((2, PIECES)),
            dma((2, PIECES)),
            dma((2, PIECES)),
        ],
        compiler_params=pltpu.CompilerParams(
            collective_id=0, has_side_effects=True, vmem_limit_bytes=60 * 1024 * 1024
        ),
    )(
        tokens, in_gain.reshape(1, width), w_glu_value, w_glu_gate, w_query, w_key, w_value,
        w_gate_conv, w_gate_attn, conv_weight, conv_gain.reshape(1, conv_local), lam,
        head_gain.reshape(1, VDIM), out_conv, out_attn,
    )


def solution(mesh):
    n_sp, n_tp = mesh.shape["sp"], mesh.shape["tp"]
    assert n_tp == 4 and n_sp % 2 == 0
    col = P(None, "tp")
    in_specs = (
        P("sp", "tp"), P(), col, col, col, col, col, col, col, col,
        P("tp"), P("tp"), P(), P("tp", None), P("tp", None),
    )
    return jax.shard_map(
        functools.partial(local, n_sp, n_tp), mesh=mesh, in_specs=in_specs,
        out_specs=P(("sp", "tp"), None), check_vma=False,
    )
```

time: 187 us -> 49.4 us (0.26); the launches traced: 185 us -> 49.2 us
  blocking collectives: 69.8 us -> 0 us
  Pallas kernels: 0 us -> 46.3 us
  waiting for transfers between devices: 43.8 us -> 0 us
  matrix products: 22.3 us -> 0 us
  between operations: 14.2 us -> 0.01 us
  other arithmetic: 10.9 us -> 0 us
  starting transfers between devices: 7.33 us -> 0 us
  local copies, waits for them, and re-layouts: 10.2 us -> 2.96 us
  loops' own time: 6.15 us -> 0 us
    all_gather x2 -> x0, blocking collectives: 50.6 us -> none  [the longest x1 25.8 us: local(): value_piece = lax.all_gather(value, 'sp', axis=0, tiled=True)]
    pallas_call x0 -> x1, Pallas kernels: none -> 46.3 us  [local(): pl.pallas_call(functools.partial(kernel, n_sp, n_tp), out_shape=jax.Shape...]
    reduce_scatter x1 -> x0, waiting for transfers between devices: 25.7 us -> none  [local(): lax.psum_scatter((jnp.dot(y_conv, out_conv, preferred_element_type=jnp.fl...]
    dot_general x22 -> x0, matrix products: 22.3 us -> none  [the longest x7 8.44 us: update(): jnp.einsum('qagcd,kacd->agcqk', query_rows, key_shard, preferred_element_...]
    psum x1 -> x0, blocking collectives: 19.1 us -> none  [local(): total_sq = lax.psum(jnp.sum(conv * conv, axis=1), 'tp')]
    all_gather x1 -> x0, waiting for transfers between devices: 17.2 us -> none  [local(): lax.all_gather(tokens, 'tp', axis=1, tiled=True).astype(jnp.float32)]
    ppermute x1 -> x0, starting transfers between devices: 7.29 us -> none  [shifted(): return lax.ppermute(x, axis, pairs)]
    another operation x9 -> x0, loops' own time: 6.15 us -> none  [the longest x1 5.67 us: local(): lax.scan(visit, start_attn, (stacked_keys, stacked_values, firsts))]
  transfers between devices with their start and end apart: 3 -> 0, of which waited for: 3 -> 0; matrix products, arithmetic and copies ran while one was open for 1% -> 0% of each run, Pallas kernels for 0% -> 0%
where the time goes in v1:
time: 49.4 us; the launch traced here: 49.2 us
  Pallas kernels  46.3 us (94%)
  local copies, waits for them, and re-layouts  2.96 us (6%)
    pallas_call x1, Pallas kernels, local(): pl.pallas_call(functools.partial(kernel, n_sp, n_tp), out_shape=jax.Shape...  46.3 us
    unnamed x1, local copies, waits for them, and re-layouts  1.67 us
    reshape x1, local copies, waits for them, and re-layouts, local(): in_gain.reshape(1, width)  1.29 us

profile of v1, /device:TPU:25, one launch (start us, length us, event | category | flops | bytes accessed | tf_op | source)
XLA Modules:
  0.0 49.2 jit_solution(5307812260352425800)
XLA Ops:
  0.0 1.3 %reshape.9.gain = bf16[1,2048]{1,0:T(2,128)(2,1)} reshape(bf16[2048]{0:T(1024)(128)(2,1)} %param.16) | data formatting | bytes 8192 | tf_op jit(solution)/shard_map/reshape | solution.py:470
  1.3 46.3 %shard_map.145 = bf16[64,2048]{1,0:T(8,128)(2,1)} custom-call(bf16[256,512]{1,0:T(8,128)(2,1)} %tok.1, bf16[1,2048]{1,0:T(2,128)(2,1)} %reshape.9.gain, bf16[2048,128]{1,0:T(8,128)(2,1)} %w_glu_value.1, bf16[2048,128]{1,0:T(8,128)(2,1)} %w_glu_gate.1, bf16[2048,256]{1,0:T(8,128)(2,1)} %w_query.1, bf16[2048,128]{1,0:T(8,128)(2,1)} %w_key.1, ...), custom_call_target="tpu_custom_call" | custom-call | tf_op jit(solution)/shard_map/pallas_call | solution.py:430
  47.6 1.7 %copy.17 = bf16[64,2048]{1,0:T(8,128)(2,1)} copy(bf16[64,2048]{1,0:T(8,128)(2,1)} %shard_map.145) | data formatting | bytes 524288

commit v2 on v1

--- a/solution.py
+++ b/solution.py
@@ -18,6 +18,8 @@
 BF16 = jnp.bfloat16
 PIECES = 4
 PAD = 32
+LANES = 128
+CHUNKS = 2
 
 
 def dot(a, b, ca=1, cb=0, precision=None):
@@ -29,8 +31,8 @@
 def kernel(
     n_sp,
     n_tp,
-    tok,
-    gain,
+    tok_hbm,
+    gain_hbm,
     w_glu_value,
     w_glu_gate,
     w_query,
@@ -38,10 +40,10 @@
     w_value,
     w_gate_conv,
     w_gate_attn,
-    taps_ref,
-    conv_gain,
-    lam,
-    head_gain,
+    taps_hbm,
+    conv_gain_hbm,
+    lam_hbm,
+    head_gain_hbm,
     out_conv,
     out_attn,
     out,
@@ -81,6 +83,15 @@
     a_sem,
     x_sem,
     b_sem,
+    gain32,
+    tok,
+    gain,
+    taps_ref,
+    conv_gain,
+    lam,
+    head_gain,
+    ga,
+    small_sem,
 ):
     rows, depth = tok.shape
     width = depth * n_tp
@@ -95,6 +106,15 @@
     mate = s + 1 - 2 * y
     has_up = s + 2 < n_sp
 
+    smalls = [
+        pltpu.make_async_copy(src, dst, small_sem.at[i])
+        for i, (src, dst) in enumerate((
+            (tok_hbm, tok), (gain_hbm, gain), (taps_hbm, taps_ref),
+            (conv_gain_hbm, conv_gain), (lam_hbm, lam), (head_gain_hbm, head_gain),
+        ))
+    ]
+    for copy in smalls:
+        copy.start()
     weights = (w_key, w_value, w_glu_value, w_glu_gate, w_query, w_gate_conv, w_gate_attn)
     spans = []
     at = 0
@@ -140,6 +160,9 @@
 
     pl.semaphore_wait(barrier, 3 + jnp.minimum(s, 2) + jnp.minimum(n_sp - 1 - s, 2))
 
+    for copy in smalls:
+        copy.wait()
+
     half = rows // 2
     across = [
         tp_copy(
@@ -163,9 +186,15 @@
     def prepare(x, owner):
         wide = x.astype(F32)
         first = pl.multiple_of(owner * depth, depth)
-        g = gain[:, pl.ds(first, depth)].astype(F32)
-        return (wide * g).astype(BF16), jnp.sum(wide * wide, axis=1, keepdims=True), first
-
+        lines = depth // LANES
+        parts = [
+            wide[:, b * LANES : (b + 1) * LANES] * gain32[pl.ds(owner * lines + b, 1), :]
+            for b in range(lines)
+        ]
+        scaled = jnp.concatenate(parts, axis=1).astype(BF16)
+        return scaled, jnp.sum(wide * wide, axis=1, keepdims=True), first
+
+    gain32[...] = gain[...].astype(F32)
     scaled, squares, first = prepare(tok[...], t)
     for copy in loads:
         copy.wait()
@@ -205,17 +234,23 @@
     def _():
         tail.start()
 
+    def chunk(j, c):
+        buf = (kbuf, vbuf)[c * 2 // CHUNKS]
+        size = buf.shape[1] * 2 // CHUNKS
+        lo = (c % (CHUNKS // 2)) * size
+        return buf.at[j, lo : lo + size]
+
     def up(j, c):
-        buf = (kbuf, vbuf)[c]
-        return sp_copy(buf.at[j], buf.at[j], up_send.at[j, c], kv_recv.at[j, c], s + 2)
+        ref = chunk(j, c)
+        return sp_copy(ref, ref, up_send.at[j, c], kv_recv.at[j, c], s + 2)
 
     def side(j, c):
-        buf = (kbuf, vbuf)[c]
-        return sp_copy(buf.at[j], buf.at[j], side_send.at[j, c], kv_recv.at[j, c], mate)
+        ref = chunk(j, c)
+        return sp_copy(ref, ref, side_send.at[j, c], kv_recv.at[j, c], mate)
 
     kbuf[s] = projected(0)
     vbuf[s] = jnp.transpose(projected(1).astype(F32)).astype(BF16)
-    for c in range(2):
+    for c in range(CHUNKS):
 
         @pl.when(has_up)
         def _():
@@ -235,6 +270,9 @@
             keep = (lane >= m * QK) & (lane < (m + 1) * QK)
             q4[2 * h + m] = jnp.where(keep, qh, 0.0).astype(BF16)
     gl[PAD:, :] = glue(0, rows).astype(F32)
+
+    gate_attn = projected(6).astype(F32)
+    ga[...] = gate_attn * jax.nn.sigmoid(gate_attn)
 
     key_pos = lax.broadcasted_iota(jnp.int32, (rows, rows), 0)
     query_pos = lax.broadcasted_iota(jnp.int32, (rows, rows), 1)
@@ -274,18 +312,56 @@
     for copy in sq_copies:
         copy.start()
 
-    def visit(j):
-        k = kbuf[j]
-        v = vbuf[j]
+    def visit(j, i, at=slice(None)):
+        scores = dot(kbuf[j], q4[i, at, :], 1, 1)
+        old = m_ref[i, :, at]
+        top = jnp.maximum(old, jnp.max(scores, axis=0, keepdims=True))
+        factor = jnp.exp(old - top)
+        e = jnp.exp(scores - top)
+        m_ref[i, :, at] = top
+        l_ref[i, :, at] = l_ref[i, :, at] * factor + jnp.sum(e, axis=0, keepdims=True)
+        o_ref[i, :, at] = o_ref[i, :, at] * factor + dot(vbuf[j], e.astype(BF16))
+
+    def mate_arrives(k):
+        for c in range(CHUNKS):
+            side(mate - 2 * k, c).wait_recv()
+
+    def visit_mate(k, at=slice(None)):
         for i in range(2 * heads):
-            scores = dot(k, q4[i], 1, 1)
-            old = m_ref[i]
-            top = jnp.maximum(old, jnp.max(scores, axis=0, keepdims=True))
-            factor = jnp.exp(old - top)
-            e = jnp.exp(scores - top)
-            m_ref[i] = top
-            l_ref[i] = l_ref[i] * factor + jnp.sum(e, axis=0, keepdims=True)
-            o_ref[i] = o_ref[i] * factor + dot(v, e.astype(BF16))
+            visit(mate - 2 * k, i, at)
+
+    maps = 2 * heads // CHUNKS
+
+    def step(i, carry):
+        k = i + 1
+        j = s - 2 * k
+        for c in range(CHUNKS):
+            up(j, c).wait_recv()
+
+            @pl.when(has_up)
+            def _():
+                up(j, c).start()
+
+            side(j, c).start()
+
+            @pl.when(k > 1)
+            def _():
+                for m in range(maps):
+                    visit(j + 2, c * maps + m)
+
+        @pl.when((k > 1) | (y == 1))
+        def _():
+            mate_arrives(k - 1)
+            visit_mate(k - 1)
+
+        return carry
+
+    lax.fori_loop(0, z, step, 0)
+
+    @pl.when(z > 0)
+    def _():
+        for i in range(2 * heads):
+            visit(s - 2 * z, i)
 
     gate_conv = projected(5).astype(F32)
     for copy in sq_copies:
@@ -300,47 +376,34 @@
         normed * jax.nn.sigmoid(normed) * (gate_conv * jax.nn.sigmoid(gate_conv))
     ).astype(BF16)
 
-    @pl.when(y == 1)
-    def _():
-        for c in range(2):
-            side(mate, c).wait_recv()
-        visit(mate)
-
-    def step(i, carry):
-        k = i + 1
-        j = s - 2 * k
-        for c in range(2):
-            up(j, c).wait_recv()
-
-            @pl.when(has_up)
-            def _():
-                up(j, c).start()
-
-            side(j, c).start()
-        visit(j)
-        other = mate - 2 * k
-        for c in range(2):
-            side(other, c).wait_recv()
-        visit(other)
-        return carry
-
-    lax.fori_loop(0, z, step, 0)
-
-    for h in range(heads):
-        first_map = o_ref[2 * h] / l_ref[2 * h]
-        second_map = o_ref[2 * h + 1] / l_ref[2 * h + 1]
-        o = first_map - lam[h] * second_map
-        n = o * lax.rsqrt(jnp.mean(o * o, axis=0, keepdims=True) + EPSILON)
-        a, b = spans[6]
-        lo = a + h * VDIM
-        gate = (acc[:, lo : lo + VDIM] * inv_rms).astype(BF16).astype(F32)
-        n = jnp.transpose(n) * head_gain[...] * HEAD_SCALE
-        at = conv_local + h * VDIM
-        ybuf[:, at : at + VDIM] = (n * (gate * jax.nn.sigmoid(gate))).astype(BF16)
+    part = rows // n_tp
+    both = 2 * part
+    far_rows = pl.ds(pl.multiple_of(p2 // 2 * both, both), both)
+    near_rows = pl.ds(pl.multiple_of(t // 2 * both, both), both)
+    more_keys = (z > 0) | (y == 1)
+
+    def finish(at):
+        for h in range(heads):
+            first_map = o_ref[2 * h, :, at] / l_ref[2 * h, :, at]
+            second_map = o_ref[2 * h + 1, :, at] / l_ref[2 * h + 1, :, at]
+            o = first_map - lam[:, h : h + 1] * second_map
+            n = o * lax.rsqrt(jnp.mean(o * o, axis=0, keepdims=True) + EPSILON)
+            n = jnp.transpose(n) * head_gain[...] * HEAD_SCALE
+            lo = h * VDIM
+            ybuf[at, conv_local + lo : conv_local + lo + VDIM] = (
+                n * ga[at, lo : lo + VDIM]
+            ).astype(BF16)
 
     for copy in out_loads:
         copy.wait()
-    part = rows // n_tp
+
+    @pl.when(more_keys)
+    def _():
+        mate_arrives(z)
+        visit_mate(z, far_rows)
+
+    finish(far_rows)
+
 
     def block(p):
         return ybuf[pl.ds(pl.multiple_of(p * part, part), part), :]
@@ -355,6 +418,11 @@
         copy = tp_copy(a_out.at[c], a_in.at[c], a_sem.at[0, c], a_sem.at[1, c], p1)
         copy.start()
         a_copies.append(copy)
+
+    @pl.when(more_keys)
+    def _():
+        visit_mate(z, near_rows)
+
     x_copies = []
     for c in range(PIECES):
         a_copies[c].wait_recv()
@@ -362,6 +430,7 @@
         copy = tp_copy(x_out.at[c], x_in.at[c], x_sem.at[0, c], x_sem.at[1, c], p2)
         copy.start()
         x_copies.append(copy)
+    finish(near_rows)
     near = jnp.concatenate([block(p1), block(t)], axis=0)
     b_copies = []
     for c in range(PIECES):
@@ -385,7 +454,7 @@
     def _():
         tail.wait_send()
 
-    for c in range(2):
+    for c in range(CHUNKS):
 
         @pl.when(has_up)
         def _():
@@ -397,7 +466,7 @@
 
     def drain(i, carry):
         j = s - 2 * (i + 1)
-        for c in range(2):
+        for c in range(CHUNKS):
 
             @pl.when(has_up)
             def _():
@@ -424,13 +493,12 @@
     cols = out_cols // PIECES
     vmem = pl.BlockSpec(memory_space=pltpu.VMEM)
     hbm = pl.BlockSpec(memory_space=pl.ANY)
-    smem = pl.BlockSpec(memory_space=pltpu.SMEM)
     dma = pltpu.SemaphoreType.DMA
     piece = pltpu.VMEM((PIECES, part, cols), BF16)
     return pl.pallas_call(
         functools.partial(kernel, n_sp, n_tp),
         out_shape=jax.ShapeDtypeStruct((part, out_cols), BF16),
-        in_specs=[vmem, vmem] + [hbm] * 7 + [vmem, vmem, smem, vmem, hbm, hbm],
+        in_specs=[hbm] * len(args),
         out_specs=vmem,
         scratch_shapes=[
             pltpu.VMEM((width, total_cols), BF16),
@@ -453,22 +521,32 @@
             dma((9,)),
             dma((5,)),
             dma((5,)),
-            dma((n_sp, 2)),
-            dma((n_sp, 2)),
-            dma((n_sp, 2)),
+            dma((n_sp, CHUNKS)),
+            dma((n_sp, CHUNKS)),
+            dma((n_sp, CHUNKS)),
             dma((2,)),
             dma((3,)),
             dma((3,)),
             dma((2, PIECES)),
             dma((2, PIECES)),
             dma((2, PIECES)),
+            pltpu.VMEM((width // LANES, LANES), F32),
+            pltpu.VMEM(tokens.shape, BF16),
+            pltpu.VMEM((width // LANES, LANES), BF16),
+            pltpu.VMEM(conv_weight.shape, BF16),
+            pltpu.VMEM((1, conv_local), F32),
+            pltpu.VMEM((1, heads), F32),
+            pltpu.VMEM((1, VDIM), F32),
+            pltpu.VMEM((rows, heads * VDIM), F32),
+            dma((6,)),
         ],
         compiler_params=pltpu.CompilerParams(
             collective_id=0, has_side_effects=True, vmem_limit_bytes=60 * 1024 * 1024
         ),
     )(
-        tokens, in_gain.reshape(1, width), w_glu_value, w_glu_gate, w_query, w_key, w_value,
-        w_gate_conv, w_gate_attn, conv_weight, conv_gain.reshape(1, conv_local), lam,
+        tokens, in_gain.reshape(width // LANES, LANES), w_glu_value, w_glu_gate, w_query, w_key, w_value,
+        w_gate_conv, w_gate_attn, conv_weight, conv_gain.reshape(1, conv_local),
+        lam.reshape(1, heads),
         head_gain.reshape(1, VDIM), out_conv, out_attn,
     )
 

time: 49.4 us -> 38.8 us (0.79); the launches traced: 49.2 us -> 38.1 us
  Pallas kernels: 46.3 us -> 36.4 us
  local copies, waits for them, and re-layouts: 2.96 us -> 1.67 us
    pallas_call x1, Pallas kernels: 46.3 us -> 36.4 us  [local(): pl.pallas_call(functools.partial(kernel, n_sp, n_tp), out_shape=jax.Shape...]
    reshape x1 -> x0, local copies, waits for them, and re-layouts: 1.29 us -> none  [local(): in_gain.reshape(1, width)]
where the time goes in v2:
time: 38.8 us; the launch traced here: 38.1 us
  Pallas kernels  36.4 us (94%)
  local copies, waits for them, and re-layouts  1.67 us (4%)
    pallas_call x1, Pallas kernels, local(): pl.pallas_call(functools.partial(kernel, n_sp, n_tp), out_shape=jax.Shape...  36.4 us
    unnamed x1, local copies, waits for them, and re-layouts  1.67 us

profile of v2, /device:TPU:25, one launch (start us, length us, event | category | flops | bytes accessed | tf_op | source)
XLA Modules:
  0.0 38.1 jit_solution(7352554549396651467)
XLA Ops:
  0.0 36.4 %shard_map.145 = bf16[64,2048]{1,0:T(8,128)(2,1)} custom-call(bf16[256,512]{1,0:T(8,128)(2,1)} %tok_hbm.1, bf16[16,128]{1,0:T(8,128)(2,1)} %bitcast.4, bf16[2048,128]{1,0:T(8,128)(2,1)} %w_glu_value.1, bf16[2048,128]{1,0:T(8,128)(2,1)} %w_glu_gate.1, bf16[2048,256]{1,0:T(8,128)(2,1)} %w_query.1, bf16[2048,128]{1,0:T(8,128)(2,1)} %w_key.1, ...), custom_call_target="tpu_custom_call" | custom-call | tf_op jit(solution)/shard_map/pallas_call | solution.py:498
  36.4 1.7 %copy.17 = bf16[64,2048]{1,0:T(8,128)(2,1)} copy(bf16[64,2048]{1,0:T(8,128)(2,1)} %shard_map.145) | data formatting | bytes 524288

commit v3 on v2

--- a/solution.py
+++ b/solution.py
@@ -51,8 +51,7 @@
     w_out,
     tokbuf,
     acc,
-    kbuf,
-    vbuf,
+    kv,
     q4,
     m_ref,
     l_ref,
@@ -94,6 +93,7 @@
     small_sem,
 ):
     rows, depth = tok.shape
+    assert rows == 2 * CHUNKS * QK
     width = depth * n_tp
     s = lax.axis_index("sp")
     t = lax.axis_index("tp")
@@ -151,14 +151,20 @@
     barrier = pltpu.get_barrier_semaphore()
     for peer in (p1, p2, p3):
         pl.semaphore_signal(barrier, inc=1, device_id={"tp": peer}, device_id_type=MESH)
-    for by in (-2, -1, 1, 2):
+    n_z = n_sp // 2
+    reach = range(2, n_sp, 4)
+    for by in [-1, 1] + [-d for d in reach] + list(reach):
         other = s + by
 
         @pl.when((other >= 0) & (other < n_sp))
         def _():
             pl.semaphore_signal(barrier, inc=1, device_id={"sp": other}, device_id_type=MESH)
 
-    pl.semaphore_wait(barrier, 3 + jnp.minimum(s, 2) + jnp.minimum(n_sp - 1 - s, 2))
+    above = (n_z - z) // 2
+    pl.semaphore_wait(
+        barrier,
+        3 + jnp.minimum(s, 1) + jnp.minimum(n_sp - 1 - s, 1) + (z + 1) // 2 + above,
+    )
 
     for copy in smalls:
         copy.wait()
@@ -203,64 +209,79 @@
     scaled, more, first = prepare(tokbuf[0], p1)
     squares = squares + more
     acc[...] += dot(scaled, w_all[pl.ds(first, depth), :])
-    for c in range(2):
-        across[c].wait_recv()
-        passed[c].start()
-    scaled, more, first = prepare(tokbuf[1], p2)
-    squares = squares + more
-    acc[...] += dot(scaled, w_all[pl.ds(first, depth), :])
-    for c in range(2):
-        passed[c].wait_recv()
-    scaled, more, first = prepare(tokbuf[2], p3)
-    squares = squares + more
-    inv_rms = lax.rsqrt(squares / width + EPSILON)
     early = spans[3][1]
-    acc[:, :early] += dot(scaled, w_all[pl.ds(first, depth), :early])
+    invs, scaled2, scaled3 = [], [], []
 
     def projected(i, lo=0, hi=None):
         hi = rows if hi is None else hi
         a, b = spans[i]
-        return (acc[lo:hi, a:b] * inv_rms[lo:hi]).astype(BF16)
+        inv = jnp.concatenate(invs, axis=0)[lo:hi]
+        return (acc[lo:hi, a:b] * inv).astype(BF16)
 
     def glue(lo, hi):
         value = projected(2, lo, hi).astype(F32)
         gate = projected(3, lo, hi).astype(F32)
         return (value * jax.nn.sigmoid(gate)).astype(BF16)
 
-    tail_out[...] = glue(rows - PAD, rows)
     tail = sp_copy(tail_out, tail_in, tail_sem.at[0], tail_sem.at[1], s + 1)
 
-    @pl.when(s + 1 < n_sp)
-    def _():
-        tail.start()
-
-    def chunk(j, c):
-        buf = (kbuf, vbuf)[c * 2 // CHUNKS]
-        size = buf.shape[1] * 2 // CHUNKS
-        lo = (c % (CHUNKS // 2)) * size
-        return buf.at[j, lo : lo + size]
-
     def up(j, c):
-        ref = chunk(j, c)
+        ref = kv.at[j, c]
         return sp_copy(ref, ref, up_send.at[j, c], kv_recv.at[j, c], s + 2)
 
+    def ahead(i, c):
+        ref = kv.at[s, c]
+        to = s + 2 + 4 * i
+        return sp_copy(ref, ref, up_send.at[to, c], kv_recv.at[s, c], to)
+
     def side(j, c):
-        ref = chunk(j, c)
+        ref = kv.at[j, c]
         return sp_copy(ref, ref, side_send.at[j, c], kv_recv.at[j, c], mate)
 
-    kbuf[s] = projected(0)
-    vbuf[s] = jnp.transpose(projected(1).astype(F32)).astype(BF16)
     for c in range(CHUNKS):
-
-        @pl.when(has_up)
-        def _():
-            up(s, c).start()
+        at = slice(c * half, (c + 1) * half)
+        across[c].wait_recv()
+        passed[c].start()
+        x2, more2, first2 = prepare(tokbuf[1, at], p2)
+        acc[at, :early] += dot(x2, w_all[pl.ds(first2, depth), :early])
+        passed[c].wait_recv()
+        x3, more3, first3 = prepare(tokbuf[2, at], p3)
+        acc[at, :early] += dot(x3, w_all[pl.ds(first3, depth), :early])
+        scaled2.append(x2)
+        scaled3.append(x3)
+        invs.append(lax.rsqrt((squares[at] + more2 + more3) / width + EPSILON))
+        if c == CHUNKS - 1:
+            tail_out[...] = glue(rows - PAD, rows)
+
+            @pl.when(s + 1 < n_sp)
+            def _():
+                tail.start()
+
+        kv[s, c, :half] = projected(0, c * half, (c + 1) * half)
+        kv[s, c, half:] = jnp.transpose(
+            projected(1, c * half, (c + 1) * half).astype(F32)
+        ).astype(BF16)
+
+        def send_ahead(i, carry):
+            ahead(i, c).start()
+            return carry
+
+        lax.fori_loop(0, above, send_ahead, 0)
 
         @pl.when(y == 0)
         def _():
             side(s, c).start()
 
-    acc[:, early:] += dot(scaled, w_all[pl.ds(first, depth), early:])
+    def keys(j):
+        return jnp.concatenate([kv[j, c, :half] for c in range(CHUNKS)], axis=0)
+
+    def values(j):
+        return jnp.concatenate([kv[j, c, half:] for c in range(CHUNKS)], axis=1)
+
+    for parts, first in ((scaled2, first2), (scaled3, first3)):
+        acc[:, early:] += dot(
+            jnp.concatenate(parts, axis=0), w_all[pl.ds(first, depth), early:]
+        )
     query = projected(4).astype(F32) * (1.0 / math.sqrt(QK))
     heads = w_query.shape[1] // (2 * QK)
     lane = lax.broadcasted_iota(jnp.int32, (rows, 2 * QK), 1)
@@ -277,8 +298,8 @@
     key_pos = lax.broadcasted_iota(jnp.int32, (rows, rows), 0)
     query_pos = lax.broadcasted_iota(jnp.int32, (rows, rows), 1)
     allowed = key_pos <= query_pos
-    k = kbuf[s]
-    v = vbuf[s]
+    k = keys(s)
+    v = values(s)
     for i in range(2 * heads):
         scores = jnp.where(allowed, dot(k, q4[i], 1, 1), NEG_BIG)
         top = jnp.max(scores, axis=0, keepdims=True)
@@ -313,14 +334,14 @@
         copy.start()
 
     def visit(j, i, at=slice(None)):
-        scores = dot(kbuf[j], q4[i, at, :], 1, 1)
+        scores = dot(keys(j), q4[i, at, :], 1, 1)
         old = m_ref[i, :, at]
         top = jnp.maximum(old, jnp.max(scores, axis=0, keepdims=True))
         factor = jnp.exp(old - top)
         e = jnp.exp(scores - top)
         m_ref[i, :, at] = top
         l_ref[i, :, at] = l_ref[i, :, at] * factor + jnp.sum(e, axis=0, keepdims=True)
-        o_ref[i, :, at] = o_ref[i, :, at] * factor + dot(vbuf[j], e.astype(BF16))
+        o_ref[i, :, at] = o_ref[i, :, at] * factor + dot(values(j), e.astype(BF16))
 
     def mate_arrives(k):
         for c in range(CHUNKS):
@@ -338,7 +359,7 @@
         for c in range(CHUNKS):
             up(j, c).wait_recv()
 
-            @pl.when(has_up)
+            @pl.when(has_up & (k % 2 == 1))
             def _():
                 up(j, c).start()
 
@@ -456,9 +477,11 @@
 
     for c in range(CHUNKS):
 
-        @pl.when(has_up)
-        def _():
-            up(s, c).wait_send()
+        def sent_ahead(i, carry):
+            ahead(i, c).wait_send()
+            return carry
+
+        lax.fori_loop(0, above, sent_ahead, 0)
 
         @pl.when(y == 0)
         def _():
@@ -468,7 +491,7 @@
         j = s - 2 * (i + 1)
         for c in range(CHUNKS):
 
-            @pl.when(has_up)
+            @pl.when(has_up & (i % 2 == 0))
             def _():
                 up(j, c).wait_send()
 
@@ -505,8 +528,7 @@
             pltpu.VMEM((out_rows, out_cols), BF16),
             pltpu.VMEM((3, rows, depth), BF16),
             pltpu.VMEM((rows, total_cols), F32),
-            pltpu.VMEM((n_sp, rows, 2 * QK), BF16),
-            pltpu.VMEM((n_sp, VDIM, rows), BF16),
+            pltpu.VMEM((n_sp, CHUNKS, rows // CHUNKS + VDIM, 2 * QK), BF16),
             pltpu.VMEM((2 * heads, rows, 2 * QK), BF16),
             pltpu.VMEM((2 * heads, 1, rows), F32),
             pltpu.VMEM((2 * heads, 1, rows), F32),

time: 38.8 us -> 40.1 us (1.034)
  Pallas kernels: 36.4 us -> 37.7 us
    pallas_call x1, Pallas kernels: 36.4 us -> 37.7 us  [local(): pl.pallas_call(functools.partial(kernel, n_sp, n_tp), out_shape=jax.Shape...]
where the time goes in v3:
time: 40.1 us; the launch traced here: 39.4 us
  Pallas kernels  37.7 us (94%)
  local copies, waits for them, and re-layouts  1.67 us (4%)
    pallas_call x1, Pallas kernels, local(): pl.pallas_call(functools.partial(kernel, n_sp, n_tp), out_shape=jax.Shape...  37.7 us
    unnamed x1, local copies, waits for them, and re-layouts  1.67 us

profile of v3, /device:TPU:25, one launch (start us, length us, event | category | flops | bytes accessed | tf_op | source)
XLA Modules:
  0.0 39.4 jit_solution(6458942522081555107)
XLA Ops:
  0.0 37.7 %shard_map.145 = bf16[64,2048]{1,0:T(8,128)(2,1)} custom-call(bf16[256,512]{1,0:T(8,128)(2,1)} %tok_hbm.1, bf16[16,128]{1,0:T(8,128)(2,1)} %bitcast.4, bf16[2048,128]{1,0:T(8,128)(2,1)} %w_glu_value.1, bf16[2048,128]{1,0:T(8,128)(2,1)} %w_glu_gate.1, bf16[2048,256]{1,0:T(8,128)(2,1)} %w_query.1, bf16[2048,128]{1,0:T(8,128)(2,1)} %w_key.1, ...), custom_call_target="tpu_custom_call" | custom-call | tf_op jit(solution)/shard_map/pallas_call | solution.py:521
  37.7 1.7 %copy.17 = bf16[64,2048]{1,0:T(8,128)(2,1)} copy(bf16[64,2048]{1,0:T(8,128)(2,1)} %shard_map.145) | data formatting | bytes 524288
